TPU v7x, 32 devices: a whole 2x2x4 slice. The times are simulated.
32 devices in a mesh: grp: 2 (over y), sp: 4 (over z), tp: 4 (over x, core).
Axes of the slice: x: 2, y: 2, z: 4, core: 2. Of those that a mesh axis runs over, the one named last changes fastest.
Arguments:
- tokens: bfloat16 [2, 2048, 2048], P('grp', ('sp', 'tp')), parts along dimension 0, may hold values from -6 to 6
- norm_gain: bfloat16 [2048], replicated, may hold values from 0.099609375 to 1.8984375
- w_query: bfloat16 [2048, 1024], P('sp'), may hold values from -0.125 to 0.125
- w_forget: bfloat16 [2048, 1024], P('sp'), may hold values from -0.125 to 0.125
- w_input: bfloat16 [2048, 1024], P('sp'), may hold values from -0.125 to 0.125
- floor_gap: float32 [1024], replicated, may hold values from 0.000146484375 to 0.12
- extra_decay: float32 [2, 2048, 16], P('grp', ('sp', 'tp')), parts along dimension 0, may hold values from -1.4 to 0, as said below
- init_state: float32 [2, 16, 64, 64], P('grp'), parts along dimension 0, may hold values from -0.078125 to 0.078125
- head_norm_gain: bfloat16 [1024], replicated, may hold values from 0.099609375 to 1.8984375
- w_output: bfloat16 [1024, 2048], P(None, 'sp'), may hold values from -0.1875 to 0.1875
Outputs:
- mixed: bfloat16 [2, 2048, 2048], P('grp', ('sp', 'tp')), parts along dimension 0
- final_state: float32 [2, 65536], P('grp', ('sp', 'tp')), parts along dimension 0
There are 2 independent parts, one for each index of `grp`. A program takes and returns all parts, laid end to end along the dimension named above; an argument that names none is the same for every part. Nothing has to cross between parts.
Inputs may be any that keep to these rules, and one draw needn't show every extreme that they name: `extra_decay`: no entry is positive.
All inputs are finite; a program needn't handle non-finite values.
Results may differ from a plain program's by a relative error of at most 0.014.
Values may be sent and summed in bfloat16 or wider, within the bound.
A program may use at most 128 MiB of HBM per device.

v0:
```python
import jax
import jax.numpy as jnp
from jax import lax
from jax.sharding import PartitionSpec as P

HEADS = 16
HEAD = 64
BLOCK = 64
EPSILON = 1e-05


def carried_in(value, axis, combine, identity):
    peers, mine = (lax.axis_size(axis), lax.axis_index(axis))
    everything = jax.tree.map(
        lambda part, kind: lax.all_gather(part.astype(kind), axis),
        value,
        (jnp.bfloat16, jnp.bfloat16),
    )
    start = jax.tree.map(
        lambda part, zero: jnp.broadcast_to(jnp.asarray(zero, part.dtype), part.shape),
        value,
        identity,
    )

    def step(k, before):
        reached = k < mine
        new = combine(
            before, jax.tree.map(lambda part, own: part[k].astype(own.dtype), everything, value)
        )
        return jax.tree.map(lambda a, b: jnp.where(reached, a, b), new, before)

    return lax.fori_loop(0, peers, step, start)


def broadcast(block, axis, source):
    block = jnp.where(lax.axis_index(axis) == source, block, jnp.zeros_like(block))
    return lax.psum(block, axis)


def layer_normed(tokens, norm_gain):
    values = tokens.astype(jnp.float32)
    center = values - jnp.mean(values, axis=-1, keepdims=True)
    spread = jnp.mean(center * center, axis=-1, keepdims=True)
    return (center * lax.rsqrt(spread + EPSILON) * norm_gain.astype(jnp.float32)).astype(
        jnp.bfloat16
    )


def gate_terms(query_sum, forget_sum, input_sum, floor_gap, extra_decay):
    query_raw = query_sum.astype(jnp.bfloat16)
    forget_raw = forget_sum.astype(jnp.bfloat16)
    input_raw = input_sum.astype(jnp.bfloat16)
    forget_pre = forget_raw.astype(jnp.float32)
    split_shape = forget_pre.shape[:-1] + (HEADS, HEAD)
    log_keep = jnp.logaddexp(
        jnp.log1p(-floor_gap), jnp.log(floor_gap) + jax.nn.log_sigmoid(forget_pre)
    )
    log_keep = log_keep.reshape(split_shape) + extra_decay[..., None]
    key_gate = (floor_gap * jax.nn.sigmoid(-forget_pre)).reshape(split_shape)
    query = jax.nn.silu(query_raw.astype(jnp.float32)).reshape(split_shape)
    values = input_raw.astype(jnp.float32).reshape(split_shape)
    return (query, key_gate, values, log_keep)


def block_pass(query, key_gate, values, log_keep):
    highest = lax.Precision.HIGHEST
    cumul = jnp.cumsum(log_keep, axis=2)
    q_decayed = query * jnp.exp(cumul)
    key_decayed = key_gate * jnp.exp(-cumul)
    causal = lax.broadcasted_iota(jnp.int32, (BLOCK, BLOCK), 0) >= lax.broadcasted_iota(
        jnp.int32, (BLOCK, BLOCK), 1
    )
    scores = jnp.einsum("snthd,snuhd->snhtu", q_decayed, key_decayed, precision=highest)
    scores = jnp.where(causal, scores, 0.0)
    within = jnp.einsum("snhtu,snuhe->snthe", scores, values, precision=highest)
    totals = cumul[:, :, -1]
    k_tail = key_gate * jnp.exp(totals[:, :, None] - cumul)
    block_state = jnp.einsum("snthd,snthe->snhde", k_tail, values, precision=highest)
    return (q_decayed, within, totals, block_state)


def linked_advance(earlier, later):
    return (earlier[0] + later[0], jnp.exp(later[0])[..., None] * earlier[1] + later[1])


def read_out(q_global, leading_logarithm, prefix_state, init_part):
    carried = jnp.exp(leading_logarithm)[..., None] * init_part + prefix_state
    added = jnp.einsum("snthd,shde->snthe", q_global, carried, precision=lax.Precision.HIGHEST)
    return (carried, added)


def body(
    tokens,
    norm_gain,
    w_query,
    w_forget,
    w_input,
    floor_gap,
    extra_decay,
    init_state,
    head_norm_gain,
    w_output,
):
    normed = layer_normed(tokens, norm_gain)
    seqs, span = (tokens.shape[0], tokens.shape[1])

    def add_rows(piece):
        return jnp.dot(normed, piece, preferred_element_type=jnp.float32)

    query_sum = add_rows(lax.all_gather(w_query, "sp", axis=0, tiled=True))
    forget_sum = add_rows(lax.all_gather(w_forget, "sp", axis=0, tiled=True))
    input_sum = add_rows(lax.all_gather(w_input, "sp", axis=0, tiled=True))
    query, key_gate, values, log_keep = gate_terms(
        query_sum, forget_sum, input_sum, floor_gap, extra_decay
    )
    blocks = span // BLOCK
    blocked = (seqs, blocks, BLOCK, HEADS, HEAD)
    q_decayed, within, totals, block_state = block_pass(
        query.reshape(blocked),
        key_gate.reshape(blocked),
        values.reshape(blocked),
        log_keep.reshape(blocked),
    )
    running_state = jnp.zeros((seqs, HEADS, HEAD, HEAD), jnp.float32)
    running_log = jnp.zeros((seqs, HEADS, HEAD), jnp.float32)
    entering_list = []
    offset_list = []
    for number in range(blocks):
        entering_list.append(running_state)
        offset_list.append(running_log)
        running_state = (
            jnp.exp(totals[:, number])[..., None] * running_state + block_state[:, number]
        )
        running_log = running_log + totals[:, number]
    entering = jnp.stack(entering_list, axis=1)
    offsets = jnp.stack(offset_list, axis=1)
    local_out = within + jnp.einsum(
        "snthd,snhde->snthe", q_decayed, entering, precision=lax.Precision.HIGHEST
    )
    q_global = q_decayed * jnp.exp(offsets[:, :, None])
    leading_logarithm, prefix_state = carried_in(
        (running_log, running_state),
        ("sp", "tp"),
        linked_advance,
        (jnp.zeros_like(running_log), jnp.zeros_like(running_state)),
    )
    carried, added = read_out(q_global, leading_logarithm, prefix_state, init_state)
    flat_total = HEADS * HEAD * HEAD
    piece_count = flat_total // lax.axis_size(("sp", "tp"))
    piece_start = lax.axis_index(("sp", "tp")) * piece_count
    after_state = (jnp.exp(running_log)[..., None] * carried + running_state).reshape(
        seqs, flat_total
    )
    whole_state = broadcast(
        after_state.astype(jnp.bfloat16), ("sp", "tp"), lax.axis_size(("sp", "tp")) - 1
    ).astype(after_state.dtype)
    final_state = lax.dynamic_slice_in_dim(whole_state, piece_start, piece_count, 1)
    recurrent = (local_out + added).reshape(seqs, span, HEADS, HEAD)
    average_power = jnp.mean(recurrent * recurrent, axis=-1, keepdims=True)
    scaled = (
        recurrent
        * lax.rsqrt(average_power + EPSILON)
        * head_norm_gain.astype(jnp.float32).reshape(HEADS, HEAD)
    )
    gated = scaled.reshape(seqs, span, HEADS * HEAD).astype(jnp.bfloat16)
    mixed = jnp.dot(
        gated,
        lax.all_gather(w_output, "sp", axis=1, tiled=True),
        preferred_element_type=jnp.float32,
    ).astype(jnp.bfloat16)
    return (mixed, final_state)


def solution(mesh):
    placed = (
        P("grp", ("sp", "tp"), None),
        P(),
        P("sp", None),
        P("sp", None),
        P("sp", None),
        P(),
        P("grp", ("sp", "tp"), None),
        P("grp", None, None, None),
        P(),
        P(None, "sp"),
    )
    return jax.shard_map(
        body,
        mesh=mesh,
        in_specs=placed,
        out_specs=(P("grp", ("sp", "tp"), None), P("grp", ("sp", "tp"))),
        check_vma=False,
    )
```

profile of v0, /device:TPU:0, one launch (start us, length us, event | category | flops | bytes accessed | tf_op | source)
XLA Modules:
  0.0 493.7 jit_solution(17431788789680109495)
XLA Ops:
  12.1 1.3 fusion.9
  13.5 79.6 %all-gather.10.cloned.1.call-done = bf16[2048,1024]{1,0:T(8,128)(2,1)} async-done(((bf16[512,1024]{1,0:T(8,128)(2,1)}), bf16[2048,1024]{1,0:T(8,128)(2,1)}) %all-gather.10.cloned.1.call-update) | async-done | bytes 4194320 | tf_op jit(solution)/shard_map/all_gather | solution.py:111
  93.1 3.7 add_select_fusion.1
  97.1 1.3 reshape_reshape.8
  98.4 75.5 %all-gather.8.cloned.1.call-done = bf16[2048,1024]{1,0:T(8,128)(2,1)} async-done(((bf16[512,1024]{1,0:T(8,128)(2,1)}), bf16[2048,1024]{1,0:T(8,128)(2,1)}) %all-gather.8.cloned.1.call-update) | async-done | bytes 4194320 | tf_op jit(solution)/shard_map/all_gather | solution.py:110
  173.9 3.0 divide_multiply_fusion.1
  178.7 76.1 %all-gather.6.cloned.1.call-done = bf16[2048,1024]{1,0:T(8,128)(2,1)} async-done(((bf16[512,1024]{1,0:T(8,128)(2,1)}), bf16[2048,1024]{1,0:T(8,128)(2,1)}) %all-gather.6.cloned.1.call-update) | async-done | bytes 4194320 | tf_op jit(solution)/shard_map/all_gather | solution.py:112
  254.8 2.9 convolution_convert_fusion.3
  258.1 3.3 fusion.18
  264.6 19.4 %all_gather.23 = bf16[16,1,16,64]{3,2,1,0:T(8,128)(2,1)S(1)} all-gather(bf16[1,1,16,64]{3,2,1,0:T(8,128)(2,1)S(1)} %get-tuple-element.162), channel_id=1, replica_groups=mesh['grp'=2,'sp'=4,'tp'=4] {'sp','tp'}, dimensions={0}, use_global_device_ids=true | all-gather | bytes 34816 | tf_op jit(solution)/shard_map/all_gather | solution.py:15
  284.0 3.6 convolution_select_fusion
  288.6 3.1 fusion.3
  291.7 21.5 %all-gather.12.cloned.1.call-done = bf16[16,1,16,64,64]{4,3,2,1,0:T(8,128)(2,1)} async-done(((bf16[1,1,16,64,64]{4,3,2,1,0:T(8,128)(2,1)}), bf16[16,1,16,64,64]{4,3,2,1,0:T(8,128)(2,1)}) %all-gather.12.cloned.1.call-update) | async-done | bytes 2097168 | tf_op jit(solution)/shard_map/all_gather | solution.py:15
  313.2 22.0 %while.16 = (s32[]{:T(128)}, f32[1,16,64]{2,1,0:T(8,128)S(1)}, f32[1,16,64,64]{3,2,1,0:T(8,128)S(1)}, s32[]{:T(128)}, bf16[16,1,16,64]{3,2,1,0:T(8,128)(2,1)S(1)...) while((s32[]{:T(128)}, f32[1,16,64]{2,1,0:T(8,128)S(1)}, ...), condition=%wide.region_4.5_spmd.clone, body=%wide.region_3.4_spmd.clone.sunk | while | flops 332804 | bytes 675959 | solution.py:32
  313.3 1.4 fusion.53
  314.7 1.3 fusion.53
  316.1 1.3 fusion.53
  317.4 1.3 fusion.53
  318.8 1.3 fusion.53
  320.2 1.3 fusion.53
  321.6 1.3 fusion.53
  322.9 1.3 fusion.53
  324.3 1.3 fusion.53
  328.4 1.3 fusion.53
  332.5 1.3 fusion.53
  333.9 1.3 fusion.53
  336.8 5.6 %multiply_reduce_fusion = (f32[2,64,16]{1,2,0:T(8,128)S(1)}, f32[1,2,64,16,64]{2,4,3,1,0:T(8,128)}) fusion(f32[1,2,64,16,64]{2,4,3,1,0:T(8,128)} %fusion.3, f32[2,64,16,64]{3,2,1,0:T(8,128)S(1)} %copy-done, f32[1,16,64,64]{3,2,1,0:T(8,128)S(1)} %get-tuple-element.113, f32[1,16,64,64]{3,2,1,0:T(8,128)S(1)} %copy-done.3, ...), kind=kOutput, calls=%fused_computation.39 | convolution fusion | flops 101185536 | bytes 2109440 | tf_op jit(solution)/shard_map/snthd,shde->snthe/dot_general | solution.py:88
  342.4 1.7 copy.56
  344.9 49.1 %all-gather.14.cloned.1.call-done = bf16[1024,2048]{1,0:T(8,128)(2,1)} async-done(((bf16[1024,512]{1,0:T(8,128)(2,1)}), bf16[1024,2048]{1,0:T(8,128)(2,1)}) %all-gather.14.cloned.1.call-update) | async-done | bytes 4194320 | tf_op jit(solution)/shard_map/all_gather | solution.py:168
  394.0 3.7 fusion.2
  397.7 87.8 %all-reduce.4.cloned.1.call-done = bf16[1,65536]{1,0:T(2,128)(2,1)} async-done(((bf16[1,65536]{1,0:T(2,128)(2,1)}), bf16[1,65536]{1,0:T(2,128)(2,1)}) %all-reduce.4.cloned.1.call-update) | async-done | bytes 131088 | tf_op jit(solution)/shard_map/psum | solution.py:37
  485.5 1.3 dynamic-slice_convert_fusion
  (89 shorter events, 19.2 us)
Async XLA Ops:
  7.2 86.0 %copy-start.2 = (bf16[1,128,2048]{2,1,0:T(8,128)(2,1)S(1)}, bf16[1,128,2048]{2,1,0:T(8,128)(2,1)}, u32[]{:S(2)}) copy-start(bf16[1,128,2048]{2,1,0:T(8,128)(2,1)} %param.12) | copy-start | bytes 1572868
  7.2 6.3 %copy-start.4 = (f32[1024]{0:T(1024)S(1)}, f32[1024]{0:T(1024)}, u32[]{:S(2)}) copy-start(f32[1024]{0:T(1024)} %param.17) | copy-start | bytes 12292
  7.2 85.9 %all-gather.10.cloned.1.call-start = ((), (), s32[]{:S(2)}) async-start(), calls=%async_computation.2 | async-start | bytes 5242880 | tf_op jit(solution)/shard_map/all_gather | solution.py:111
  7.9 166.0 %all-gather.8.cloned.1.call-start = ((), (), s32[]{:S(2)}) async-start(), calls=%async_computation.1 | async-start | bytes 5242880 | tf_op jit(solution)/shard_map/all_gather | solution.py:110
  8.7 246.1 %all-gather.6.cloned.1.call-start = ((), (), s32[]{:S(2)}) async-start(), calls=%async_computation | async-start | bytes 5242880 | tf_op jit(solution)/shard_map/all_gather | solution.py:112
  9.4 303.8 %all-gather.12.cloned.1.call-start = ((), (), s32[]{:S(2)}) async-start(), calls=%async_computation.3 | async-start | bytes 4456448 | tf_op jit(solution)/shard_map/all_gather | solution.py:15
  261.5 3.1 copy-start.5
  263.9 130.1 %all-gather.14.cloned.1.call-start = ((), (), s32[]{:S(2)}) async-start(), calls=%async_computation.4 | async-start | bytes 5242880 | tf_op jit(solution)/shard_map/all_gather | solution.py:168
  264.5 221.0 %all-reduce.4.cloned.1.call-start = ((), (), s32[]{:S(2)}) async-start(), calls=%async_computation.5 | async-start | bytes 524288 | tf_op jit(solution)/shard_map/psum | solution.py:37
  264.6 24.0 %copy-start.1 = (f32[1,1,16,64,64]{4,3,2,1,0:T(8,128)S(1)}, f32[1,1,16,64,64]{4,3,2,1,0:T(8,128)}, u32[]{:S(2)}) copy-start(f32[1,1,16,64,64]{4,3,2,1,0:T(8,128)} %get-tuple-element.148) | copy-start | bytes 786436
  291.7 43.5 %copy-start.3 = (f32[1,16,64,64]{3,2,1,0:T(8,128)S(1)}, f32[1,16,64,64]{3,2,1,0:T(8,128)}, u32[]{:S(2)}) copy-start(f32[1,16,64,64]{3,2,1,0:T(8,128)} %param.19) | copy-start | bytes 786436
  313.2 23.6 %copy-start = (f32[2,64,16,64]{3,2,1,0:T(8,128)S(1)}, f32[2,64,16,64]{3,2,1,0:T(8,128)}, u32[]{:S(2)}) copy-start(f32[2,64,16,64]{3,2,1,0:T(8,128)} %get-tuple-element.153) | copy-start | bytes 1572868
Sparse Core Ops, SparseCore 0:
  9.6 83.5 all-gather.9
  94.7 79.2 all-gather.7
  175.5 79.2 all-gather.5
  264.0 49.1 all-gather.11
  314.7 79.2 all-gather.13
  397.2 88.2 all-reduce.3
where the time goes:
time: 495 us; the launch traced here: 494 us
  waiting for transfers between devices  392 us (79%)
  other arithmetic  31.6 us (6%)
  matrix products  27.9 us (6%)
  blocking collectives  19.4 us (4%)
  between operations  14.3 us (3%)
  local copies, waits for them, and re-layouts  7.27 us (1%)
    psum x1, waiting for transfers between devices, broadcast(): return lax.psum(block, axis)  87.8 us
    all_gather x1, waiting for transfers between devices, body(): forget_sum = add_rows(lax.all_gather(w_forget, 'sp', axis=0, tiled=True))  79.6 us
    all_gather x1, waiting for transfers between devices, body(): input_sum = add_rows(lax.all_gather(w_input, 'sp', axis=0, tiled=True))  76.1 us
    all_gather x1, waiting for transfers between devices, body(): query_sum = add_rows(lax.all_gather(w_query, 'sp', axis=0, tiled=True))  75.5 us
    all_gather x1, waiting for transfers between devices, body(): lax.all_gather(w_output, 'sp', axis=1, tiled=True)  49.1 us
    all_gather x1, waiting for transfers between devices, carried_in(): lax.all_gather(part.astype(kind), axis)  21.5 us
    select_n x32, other arithmetic, step(): return jax.tree.map(lambda a, b: jnp.where(reached, a, b), new, before)  21.1 us
    all_gather x1, blocking collectives, carried_in(): lax.all_gather(part.astype(kind), axis)  19.4 us
  transfers between devices with their start and end apart: 6, of which 6 were waited for; matrix products, arithmetic and copies ran while one was open for 11% of the time, Pallas kernels for 0%

commit v1 on v0

--- a/solution.py
+++ b/solution.py
@@ -34,7 +34,7 @@
 
 def broadcast(block, axis, source):
     block = jnp.where(lax.axis_index(axis) == source, block, jnp.zeros_like(block))
-    return lax.psum(block, axis)
+    return jnp.sum(lax.all_gather(block, axis), axis=0)
 
 
 def layer_normed(tokens, norm_gain):

time: 495 us -> 459 us (0.927)
  waiting for transfers between devices: 392 us -> 354 us
  other arithmetic: 31.6 us -> 37.9 us
    psum x1 -> x0, waiting for transfers between devices: 87.8 us -> none  [broadcast(): return lax.psum(block, axis)]
    all_gather x0 -> x1, waiting for transfers between devices: none -> 47.2 us  [broadcast(): return jnp.sum(lax.all_gather(block, axis), axis=0)]
    all_gather x1, waiting for transfers between devices: 21.5 us -> 29.4 us  [carried_in(): lax.all_gather(part.astype(kind), axis)]
    reduce_sum x0 -> x1, other arithmetic: none -> 5.99 us  [broadcast(): return jnp.sum(lax.all_gather(block, axis), axis=0)]
    all_gather x1, waiting for transfers between devices: 49.1 us -> 43.5 us  [body(): lax.all_gather(w_output, 'sp', axis=1, tiled=True)]
  transfers between devices with their start and end apart: 6 -> 6, of which waited for: 6 -> 6; matrix products, arithmetic and copies ran while one was open for 11% -> 12% of each run, Pallas kernels for 0% -> 0%
where the time goes in v1:
time: 459 us; the launch traced here: 458 us
  waiting for transfers between devices  354 us (77%)
  other arithmetic  37.9 us (8%)
  matrix products  25.8 us (6%)
  blocking collectives  19.2 us (4%)
  between operations  14.4 us (3%)
  local copies, waits for them, and re-layouts  6.09 us (1%)
    all_gather x1, waiting for transfers between devices, body(): forget_sum = add_rows(lax.all_gather(w_forget, 'sp', axis=0, tiled=True))  79.6 us
    all_gather x1, waiting for transfers between devices, body(): input_sum = add_rows(lax.all_gather(w_input, 'sp', axis=0, tiled=True))  76.1 us
    all_gather x1, waiting for transfers between devices, body(): query_sum = add_rows(lax.all_gather(w_query, 'sp', axis=0, tiled=True))  75.5 us
    all_gather x1, waiting for transfers between devices, broadcast(): return jnp.sum(lax.all_gather(block, axis), axis=0)  47.2 us
    all_gather x1, waiting for transfers between devices, body(): lax.all_gather(w_output, 'sp', axis=1, tiled=True)  43.5 us
    all_gather x1, waiting for transfers between devices, carried_in(): lax.all_gather(part.astype(kind), axis)  29.4 us
    select_n x32, other arithmetic, step(): return jax.tree.map(lambda a, b: jnp.where(reached, a, b), new, before)  21 us
    all_gather x1, blocking collectives, carried_in(): lax.all_gather(part.astype(kind), axis)  19.2 us
  transfers between devices with their start and end apart: 6, of which 6 were waited for; matrix products, arithmetic and copies ran while one was open for 12% of the time, Pallas kernels for 0%

profile of v1, /device:TPU:0, one launch (start us, length us, event | category | flops | bytes accessed | tf_op | source)
XLA Modules:
  0.0 458.2 jit_solution(1221731218433785744)
XLA Ops:
  12.1 1.3 fusion.9
  13.5 79.6 %all-gather.11.cloned.1.call-done = bf16[2048,1024]{1,0:T(8,128)(2,1)} async-done(((bf16[512,1024]{1,0:T(8,128)(2,1)}), bf16[2048,1024]{1,0:T(8,128)(2,1)}) %all-gather.11.cloned.1.call-update) | async-done | bytes 4194320 | tf_op jit(solution)/shard_map/all_gather | solution.py:111
  93.1 3.7 add_select_fusion.1
  97.1 1.3 reshape_reshape.8
  98.4 75.5 %all-gather.9.cloned.1.call-done = bf16[2048,1024]{1,0:T(8,128)(2,1)} async-done(((bf16[512,1024]{1,0:T(8,128)(2,1)}), bf16[2048,1024]{1,0:T(8,128)(2,1)}) %all-gather.9.cloned.1.call-update) | async-done | bytes 4194320 | tf_op jit(solution)/shard_map/all_gather | solution.py:110
  173.9 3.0 divide_multiply_fusion.1
  178.7 76.1 %all-gather.7.cloned.1.call-done = bf16[2048,1024]{1,0:T(8,128)(2,1)} async-done(((bf16[512,1024]{1,0:T(8,128)(2,1)}), bf16[2048,1024]{1,0:T(8,128)(2,1)}) %all-gather.7.cloned.1.call-update) | async-done | bytes 4194320 | tf_op jit(solution)/shard_map/all_gather | solution.py:112
  254.8 2.9 convolution_convert_fusion.3
  258.1 3.3 fusion.18
  264.6 19.2 %all_gather.27 = bf16[16,1,16,64]{3,2,1,0:T(8,128)(2,1)S(1)} all-gather(bf16[1,1,16,64]{3,2,1,0:T(8,128)(2,1)S(1)} %get-tuple-element.162), channel_id=1, replica_groups=mesh['grp'=2,'sp'=4,'tp'=4] {'sp','tp'}, dimensions={0}, use_global_device_ids=true | all-gather | bytes 34816 | tf_op jit(solution)/shard_map/all_gather | solution.py:15
  283.7 29.4 %all-gather.13.cloned.1.call-done = bf16[16,1,16,64,64]{4,3,2,1,0:T(8,128)(2,1)} async-done(((bf16[1,1,16,64,64]{4,3,2,1,0:T(8,128)(2,1)}), bf16[16,1,16,64,64]{4,3,2,1,0:T(8,128)(2,1)}) %all-gather.13.cloned.1.call-update) | async-done | bytes 2097168 | tf_op jit(solution)/shard_map/all_gather | solution.py:15
  313.1 21.9 %while.16 = (s32[]{:T(128)}, f32[1,16,64]{2,1,0:T(8,128)S(1)}, f32[1,16,64,64]{3,2,1,0:T(8,128)S(1)}, s32[]{:T(128)}, bf16[16,1,16,64]{3,2,1,0:T(8,128)(2,1)S(1)...) while((s32[]{:T(128)}, f32[1,16,64]{2,1,0:T(8,128)S(1)}, ...), condition=%wide.region_4.5_spmd.clone, body=%wide.region_3.4_spmd.clone.sunk | while | flops 332804 | bytes 675959 | solution.py:32
  313.1 1.3 fusion.53
  314.5 1.3 fusion.53
  315.9 1.3 fusion.53
  317.2 1.3 fusion.53
  318.6 1.3 fusion.53
  320.0 1.3 fusion.53
  321.4 1.3 fusion.53
  322.7 1.3 fusion.53
  324.1 1.3 fusion.53
  328.2 1.3 fusion.53
  332.3 1.3 fusion.53
  333.7 1.3 fusion.53
  335.0 1.9 fusion.37
  337.9 3.7 convolution_select_fusion
  342.6 3.1 fusion.3
  345.8 3.4 multiply_reduce_fusion
  350.3 43.5 %all-gather.15.cloned.1.call-done = bf16[1024,2048]{1,0:T(8,128)(2,1)} async-done(((bf16[1024,512]{1,0:T(8,128)(2,1)}), bf16[1024,2048]{1,0:T(8,128)(2,1)}) %all-gather.15.cloned.1.call-update) | async-done | bytes 4194320 | tf_op jit(solution)/shard_map/all_gather | solution.py:168
  393.8 3.7 fusion.2
  397.6 47.2 %all-gather.17.cloned.1.call-done = bf16[16,1,65536]{2,1,0:T(2,128)(2,1)} async-done(((bf16[1,1,65536]{2,1,0:T(2,128)(2,1)}), bf16[16,1,65536]{2,1,0:T(2,128)(2,1)}) %all-gather.17.cloned.1.call-update) | async-done | bytes 2097168 | tf_op jit(solution)/shard_map/all_gather | solution.py:37
  444.8 6.0 %reduce_sum.42 = bf16[65536]{0:T(1024)(128)(2,1)S(1)} reduce(bf16[16,1,65536]{2,1,0:T(2,128)(2,1)} %all-gather.17.cloned.1.call-done, bf16[]{:T(256)} %constant.65.clone.1), dimensions={0,1}, to_apply=%region_6.7 | reduce | flops 983040 | bytes 2228226 | tf_op jit(solution)/shard_map/reduce_sum | solution.py:37
  (88 shorter events, 19.6 us)
Async XLA Ops:
  7.2 86.0 %copy-start.1 = (bf16[1,128,2048]{2,1,0:T(8,128)(2,1)S(1)}, bf16[1,128,2048]{2,1,0:T(8,128)(2,1)}, u32[]{:S(2)}) copy-start(bf16[1,128,2048]{2,1,0:T(8,128)(2,1)} %param.12) | copy-start | bytes 1572868
  7.2 6.3 %copy-start.3 = (f32[1024]{0:T(1024)S(1)}, f32[1024]{0:T(1024)}, u32[]{:S(2)}) copy-start(f32[1024]{0:T(1024)} %param.17) | copy-start | bytes 12292
  7.2 85.9 %all-gather.11.cloned.1.call-start = ((), (), s32[]{:S(2)}) async-start(), calls=%async_computation.2 | async-start | bytes 5242880 | tf_op jit(solution)/shard_map/all_gather | solution.py:111
  7.9 166.0 %all-gather.9.cloned.1.call-start = ((), (), s32[]{:S(2)}) async-start(), calls=%async_computation.1 | async-start | bytes 5242880 | tf_op jit(solution)/shard_map/all_gather | solution.py:110
  8.7 246.1 %all-gather.7.cloned.1.call-start = ((), (), s32[]{:S(2)}) async-start(), calls=%async_computation | async-start | bytes 5242880 | tf_op jit(solution)/shard_map/all_gather | solution.py:112
  9.4 303.7 %all-gather.13.cloned.1.call-start = ((), (), s32[]{:S(2)}) async-start(), calls=%async_computation.3 | async-start | bytes 4456448 | tf_op jit(solution)/shard_map/all_gather | solution.py:15
  263.9 130.0 %all-gather.15.cloned.1.call-start = ((), (), s32[]{:S(2)}) async-start(), calls=%async_computation.4 | async-start | bytes 5242880 | tf_op jit(solution)/shard_map/all_gather | solution.py:168
  264.5 180.3 %all-gather.17.cloned.1.call-start = ((), (), s32[]{:S(2)}) async-start(), calls=%async_computation.5 | async-start | bytes 4456448 | tf_op jit(solution)/shard_map/all_gather | solution.py:37
  313.1 24.7 %copy-start.4 = (bf16[1024]{0:T(1024)(128)(2,1)S(1)}, bf16[1024]{0:T(1024)(128)(2,1)}, u32[]{:S(2)}) copy-start(bf16[1024]{0:T(1024)(128)(2,1)} %param.20) | copy-start | bytes 6148
  337.8 7.9 %copy-start = (f32[2,64,16,64]{3,2,1,0:T(8,128)S(1)}, f32[2,64,16,64]{3,2,1,0:T(8,128)}, u32[]{:S(2)}) copy-start(f32[2,64,16,64]{3,2,1,0:T(8,128)} %get-tuple-element.153) | copy-start | bytes 1572868
  337.9 7.9 %copy-start.2 = (f32[1,16,64,64]{3,2,1,0:T(8,128)S(1)}, f32[1,16,64,64]{3,2,1,0:T(8,128)}, u32[]{:S(2)}) copy-start(f32[1,16,64,64]{3,2,1,0:T(8,128)} %param.19) | copy-start | bytes 786436
Sparse Core Ops, SparseCore 0:
  9.6 83.5 all-gather.10
  94.7 79.2 all-gather.8
  175.5 79.2 all-gather.6
  264.0 49.0 all-gather.12
  314.5 79.2 all-gather.14
  395.9 48.8 all-gather.16
